TPU v7x, 32 devices: a whole 2x2x4 slice. The times are simulated.
32 devices in a mesh: sp: 8 (over z, y), tp: 4 (over x, core).
Axes of the slice: x: 2, y: 2, z: 4, core: 2. Of those that a mesh axis runs over, the one named last changes fastest.
Arguments:
- inputs: bfloat16 [8192, 2048], P('sp'), may hold values from -6 to 6
- norm_gain: float32 [3, 2048], replicated, may hold values from 0.1 to 1.9
- query_weight: bfloat16 [3, 2048, 1024], P(None, 'sp', 'tp'), may hold values from -64 to 64
- key_weight: bfloat16 [3, 2048, 512], P(None, 'sp', 'tp'), may hold values from -4 to 4
- value_weight: bfloat16 [3, 2048, 512], P(None, 'sp', 'tp'), may hold values from -0.125 to 0.125
- output_weight: bfloat16 [3, 2048, 1024], P(None, 'sp', 'tp'), may hold values from -0.1875 to 0.1875
- sink_logit: float32 [3, 16], P(None, 'tp'), may hold values from 2 to 7
- final_gain: float32 [2048], replicated, may hold values from 0.1 to 1.9
Outputs:
- result: float32 [8192, 2048], P(('sp', 'tp'))
All inputs are finite; a program needn't handle non-finite values.
Results may differ from a plain program's by a relative error of at most 0.015.
Values may be sent and summed in bfloat16 or wider, within the bound.
A program may use at most 64 MiB of HBM per device.

v0:
```python
import functools
import math

import jax
import jax.numpy as jnp
from jax import lax
from jax.experimental import pallas as pl
from jax.experimental.pallas import tpu as pltpu
from jax.sharding import PartitionSpec as P

HEAD_DIM = 64
WINDOW = 128
EPS = 1e-06
LANES = 128
F32 = jnp.float32
BF16 = jnp.bfloat16
VMEM_LIMIT = 60 * 1024 * 1024
KINDS = 3
SPLIT = 4
AHEAD = 2
LAGS = (0, 1, 2, 3, 4, 5)
SLOTS = (0, 1, 0, 1)
LATE = (1, 1, 1, 1)
LATE_FROM = 0.75
SETTLE = 4
WHOLE = slice(None)
LINE = 4


def grid_of(mesh):
    n_sp, n_tp = mesh.shape["sp"], mesh.shape["tp"]
    devices = mesh.devices
    n_z = len({d.coords[2] for d in devices[:, 0]})
    n_x = len({d.coords[0] for d in devices[0, :]})
    return n_z, n_sp // n_z, n_x, n_tp // n_x


def unit_list(layers, rows):
    units = []
    n = 0
    for layer in range(layers):
        for kind in range(KINDS):
            for piece in range(SPLIT):
                size = rows // SPLIT
                if layer == 0 and kind < 2:
                    orders = (("z", "y"), ("z", "y"))
                else:
                    orders = FLAVOURS[PATTERN[n % len(PATTERN)]]
                    n += 1
                units.append((layer, kind, piece * size, size, orders))
    return units


FLAVOURS = {
    "a": (("z", "y", "x"), ("z", "x", "y")),
    "b": (("y", "z", "x"), ("x", "z", "y")),
    "A": (("z", "y", "x"), ("z", "y", "x")),
    "B": (("y", "z", "x"), ("y", "z", "x")),
    "c": (("y", "x", "z"), ("x", "y", "z")),
    "e": (("z", "y", "x"), ("x", "z", "y")),
    "f": (("y", "z", "x"), ("z", "x", "y")),
}
PATTERN = "Abbabbabbabbab"


def normalize(wide, gain):
    inv_root = lax.rsqrt(jnp.mean(wide * wide, axis=-1, keepdims=True) + EPS)
    return wide * inv_root * gain


def finish_kernel(state_ref, gain_ref, out_ref):
    out_ref[...] = normalize(state_ref[...].astype(F32), gain_ref[...])


def stack_kernel(grid, sources, units, *refs):
    n_z, n_y, n_x, n_c = grid
    n_sp, n_tp = n_z * n_y, n_x * n_c
    (inputs_ref, gain_ref, sink_ref, inverse_ref), refs = refs[:4], refs[4:]
    weight_refs, refs = refs[: len(sources)], refs[len(sources) :]
    out_ref, refs = refs[0], refs[1:]
    w, stage_in, state, normed, queries, kv0, kv, mine, attended, bias, trig, tables, sinks = refs[:13]
    send_sem, recv_sem, halo_send, halo_recv, slice_send, slice_recv, sink_send, sink_recv, local_sem = refs[13:]

    layers, rows, cols = w.shape[1], w.shape[6], w.shape[7]
    tokens, features = state.shape
    span = n_tp * tokens
    heads = cols // HEAD_DIM
    groups = heads // 2
    kv_cols = cols // 2
    per_group = heads // groups
    blocks = tokens // WINDOW

    sp, tp = lax.axis_index("sp"), lax.axis_index("tp")
    place = sp * n_tp + tp
    z, y, x, core = sp // n_y, sp % n_y, tp // n_c, tp % n_c
    at = {"z": z, "y": y, "x": x}
    size = {"z": n_z, "y": n_y, "x": n_x}
    other = 1 - core

    def device(**where):
        to = dict(at, core=core)
        to.update(where)
        return {"sp": to["z"] * n_y + to["y"], "tp": to["x"] * n_c + to["core"]}

    def linear(index):
        return {"sp": index // n_tp, "tp": index % n_tp}

    def send(src, dst, send_at, recv_at, to):
        return pltpu.make_async_remote_copy(
            src_ref=src, dst_ref=dst, send_sem=send_at, recv_sem=recv_at,
            device_id=to, device_id_type=pl.DeviceIdType.MESH,
        )

    base = {"z": 0, "y": n_z - 1, "x": n_z + n_y - 2}
    hops = n_z + n_y + n_x - 3
    per_unit = hops + 1 + max(size.values())

    def relayed(axis):
        return axis == "z" and size[axis] == LINE

    def block(u, colour, **where):
        layer, kind, first, count, _ = units[u]
        spot = dict({"z": z, "y": y, "x": x}, **where)
        return w.at[kind, layer, spot["x"], colour, spot["z"], spot["y"], pl.ds(first, count)]

    def part(u, colour, stage, source):
        order = units[u][4][colour]
        spot = {a: WHOLE for a in order[:stage]}
        spot[order[stage]] = source
        return block(u, colour, **spot)

    def staged(u, colour, stage, k, arriving):
        axis = units[u][4][colour][stage]
        view = part(u, colour, stage, (at[axis] + size[axis] - k) % size[axis] if arriving else at[axis])
        number = u * per_unit + base[axis] + k - 1
        to = device(**{axis: (at[axis] + k) % size[axis]})
        return send(view, view, send_sem.at[number], recv_sem.at[number], to)

    def relay(u, colour, stage, inner):
        source, target = (LINE - 1, 0) if inner == 1 else (0, LINE - 1)
        view = part(u, colour, stage, source)
        number = u * per_unit
        k = (target - source) % LINE
        return send(view, view, send_sem.at[number + hops], recv_sem.at[number + k - 1], device(z=target))

    def shared(u, colour, k):
        axis = units[u][4][colour][2]
        view = part(u, colour, 2, (at[axis] + size[axis] - k) % size[axis])
        number = u * per_unit + hops + 1 + k
        return send(view, view, send_sem.at[number], recv_sem.at[number], device(core=other))

    def outgoing(u, colour, stage, do):
        axis = units[u][4][colour][stage]
        if relayed(axis):
            do(staged(u, colour, stage, 2, False))
            pl.when(z != LINE - 1)(lambda: do(staged(u, colour, stage, 1, False)))
            pl.when(z != 0)(lambda: do(staged(u, colour, stage, 3, False)))
        else:
            for k in range(1, size[axis]):
                do(staged(u, colour, stage, k, False))

    def by_core(do):
        for colour in range(n_c):
            pl.when(core == colour)(functools.partial(do, colour))

    def depart(u):
        by_core(lambda colour: outgoing(u, colour, 0, lambda c: c.start()))

    def pass_on(u, stage):
        def do(colour):
            order = units[u][4][colour]
            if stage < len(order) and relayed(order[stage]):
                staged(u, colour, stage, 2, True).wait_recv()
                for inner in (1, 2):
                    pl.when(z == inner)(lambda: relay(u, colour, stage, inner).start())
        by_core(do)

    def advance(u, stage):
        def do(colour):
            order = units[u][4][colour]
            if stage >= len(order):
                return
            axis = order[stage]
            for k in range(1, size[axis]):
                if not (relayed(axis) and k == 2):
                    staged(u, colour, stage, k, True).wait_recv()
            if stage + 1 < len(order):
                outgoing(u, colour, stage + 1, lambda c: c.start())
            if stage == 1 and len(order) == 3:
                shared(u, colour, 0).start()
            if stage == 2:
                for k in range(1, size[axis]):
                    shared(u, colour, k).start()
        by_core(do)

    def wait_shared(u):
        def do(colour):
            order = units[u][4][1 - colour]
            if len(order) == 3:
                for k in range(size[order[2]]):
                    shared(u, 1 - colour, k).wait_recv()
        by_core(do)

    def drain(u):
        def do(colour):
            order = units[u][4][colour]
            for stage, axis in enumerate(order):
                outgoing(u, colour, stage, lambda c: c.wait_send())
                if relayed(axis):
                    for inner in (1, 2):
                        pl.when(z == inner)(lambda: relay(u, colour, stage, inner).wait_send())
            if len(order) == 3:
                for k in range(size[order[2]]):
                    shared(u, colour, k).wait_send()
        by_core(do)

    own = []
    for i, (kind, offset, width) in enumerate(sources):
        dst = w.at[kind, :, x, core, z, y, :, pl.ds(offset, width)]
        own.append(pltpu.make_async_copy(weight_refs[i], dst, local_sem.at[i]))
    for copy in own:
        copy.start()

    def fetch(i):
        return pltpu.make_async_copy(
            inputs_ref.at[pl.ds(i * tokens, tokens)], stage_in.at[i % 2], local_sem.at[len(sources) + i]
        )

    for i in range(2):
        fetch(i).start()

    barrier = pltpu.get_barrier_semaphore()

    def greet(to):
        pl.semaphore_signal(barrier, inc=1, device_id=to, device_id_type=pl.DeviceIdType.MESH)

    everyone = n_sp * n_tp
    met = [device(**{axis: (at[axis] + k) % size[axis]}) for axis in ("z", "y", "x") for k in range(1, size[axis])]
    met += [{"sp": sp, "tp": (tp + k) % n_tp} for k in range(1, n_tp)]
    met += [linear((place + step) % everyone) for step in (1, everyone - 1)]
    met += [{"sp": (sp + step) % n_sp, "tp": tp} for step in (1, n_sp - 1)]
    for to in met:
        greet(to)
    for copy in own:
        copy.wait()
    pl.semaphore_wait(barrier, len(met))

    count = len(units)
    for u in range(AHEAD):
        depart(u)

    def sink_copy(k, arriving):
        source = (tp + n_tp - k) % n_tp if arriving else tp
        to = {"sp": sp, "tp": (tp + k) % n_tp}
        return send(sink_ref, sinks.at[source], sink_send.at[k - 1], sink_recv.at[k - 1], to)

    for k in range(1, n_tp):
        sink_copy(k, False).start()
    sinks[tp] = sink_ref[...]

    root = HEAD_DIM ** (-0.5)
    scale = float(features) ** (-0.5)

    def fill(i, carry):
        first = sp * span + i * WINDOW
        where = lax.broadcasted_iota(jnp.int32, (WINDOW, 2 * HEAD_DIM), 0) + first
        angles = where.astype(F32) * inverse_ref[...]
        column = lax.broadcasted_iota(jnp.int32, (WINDOW, 2 * HEAD_DIM), 1)
        sine = jnp.sin(angles)
        turned = jnp.where(column < HEAD_DIM + HEAD_DIM // 2, -sine, sine)
        trig[pl.ds(pl.multiple_of(i * WINDOW, WINDOW), WINDOW)] = (
            jnp.where(column < HEAD_DIM, jnp.cos(angles), turned) * scale
        )
        return carry

    lax.fori_loop(0, span // WINDOW, fill, 0)

    def turn_tables(kind, where):
        pair_c, pair_s = trig[where, :HEAD_DIM], trig[where, HEAD_DIM:]
        if kind:
            return jnp.concatenate([pair_c * root] * heads, axis=1), jnp.concatenate([pair_s * root] * heads, axis=1)
        one = jnp.ones((tokens, kv_cols), F32)
        return jnp.concatenate([pair_c] * groups + [one], axis=1), jnp.concatenate([pair_s] * groups + [0 * one], axis=1)

    for kind in range(2):
        tables[2 * kind], tables[2 * kind + 1] = turn_tables(kind, pl.ds(pl.multiple_of(tp * tokens, tokens), tokens))
    reach_of = 3 * WINDOW
    row = lax.broadcasted_iota(jnp.int32, (WINDOW, reach_of), 0)
    reach = lax.broadcasted_iota(jnp.int32, (WINDOW, reach_of), 1) - WINDOW
    for b in range(span // WINDOW):
        key_pos = sp * span + b * WINDOW + reach
        allowed = (jnp.abs(row - reach) <= WINDOW) & (key_pos >= 0) & (key_pos < n_sp * span)
        bias[b] = jnp.where(allowed, 0.0, -jnp.inf).astype(F32)

    has_low, has_high = place > 0, place < everyone - 1
    span_low, span_high = sp > 0, sp < n_sp - 1
    nothing = jnp.zeros((layers - 1, n_tp, WINDOW, cols), BF16)

    @pl.when(jnp.logical_not(has_low))
    def _():
        kv[:, :, :WINDOW] = nothing

    @pl.when(jnp.logical_not(has_high))
    def _():
        kv[:, :, WINDOW + tokens :] = nothing

    @pl.when(jnp.logical_not(span_low))
    def _():
        kv0[:WINDOW] = nothing[0, 0]

    @pl.when(jnp.logical_not(span_high))
    def _():
        kv0[WINDOW + span :] = nothing[0, 0]

    def halo(layer, t, up):
        length = span if layer == 0 else tokens
        here = pl.ds(length, WINDOW) if up else pl.ds(WINDOW, WINDOW)
        there = pl.ds(0, WINDOW) if up else pl.ds(WINDOW + length, WINDOW)
        number = (layer * n_tp + t) * 2 + int(up)
        rows_of = kv0 if layer == 0 else kv.at[layer - 1, t]
        step = 1 if up else -1
        to = {"sp": sp + step, "tp": tp} if layer == 0 else linear(place + step)
        return send(rows_of.at[here], rows_of.at[there], halo_send.at[number], halo_recv.at[number], to)

    def low_high(layer):
        return (span_low, span_high) if layer == 0 else (has_low, has_high)

    def send_halo(layer, t):
        low, high = low_high(layer)
        pl.when(low)(lambda: halo(layer, t, False).start())
        pl.when(high)(lambda: halo(layer, t, True).start())

    def wait_halo(layer, t):
        low, high = low_high(layer)
        pl.when(low)(lambda: halo(layer, t, True).wait_recv())
        pl.when(high)(lambda: halo(layer, t, False).wait_recv())

    def norm0(i):
        fetch(i).wait()
        normed[i] = normalize(stage_in[i % 2].astype(F32), gain_ref[0:1]).astype(BF16)
        if i + 2 < n_tp:
            fetch(i + 2).start()

    def norm(layer):
        normed[0] = normalize(state[...].astype(F32), gain_ref[layer : layer + 1]).astype(BF16)

    lane = lax.broadcasted_iota(jnp.int32, (tokens, cols), 1)
    front = (lane % HEAD_DIM) < HEAD_DIM // 2

    def project(chunk, weight, cos_table, sin_table):
        acc = jnp.dot(normed[chunk], weight.reshape(features, cols), preferred_element_type=F32)
        step = HEAD_DIM // 2
        partner = jnp.where(front, pltpu.roll(acc, cols - step, 1), pltpu.roll(acc, step, 1))
        return (acc * cos_table + partner * sin_table).astype(BF16)

    def make_kv0(i):
        kv0[WINDOW + i * tokens : WINDOW + (i + 1) * tokens] = project(
            i, w[0, 0, x, core], *turn_tables(0, pl.ds(i * tokens, tokens))
        )

    def make_q0(i):
        queries[i] = project(i, w[1, 0, x, core], *turn_tables(1, pl.ds(i * tokens, tokens)))

    def make_kv(layer, t):
        kv[layer - 1, t, WINDOW : WINDOW + tokens] = project(0, w[0, layer, t // n_c, t % n_c], tables[0], tables[1])

    def make_q(layer, t):
        queries[t] = project(0, w[1, layer, t // n_c, t % n_c], tables[2], tables[3])

    row_head = lax.broadcasted_iota(jnp.int32, (per_group * WINDOW, 1), 0) // WINDOW

    def attend_block(layer, q_ref, kv_ref, here, near, near_bias, sink_row, out):
        near_bias = jnp.concatenate([near_bias] * per_group, axis=0)
        for g in range(groups):
            first = g * per_group
            k = kv_ref[near, g * HEAD_DIM : (g + 1) * HEAD_DIM]
            v = kv_ref[near, kv_cols + g * HEAD_DIM : kv_cols + (g + 1) * HEAD_DIM]
            q = jnp.concatenate(
                [q_ref[here, h * HEAD_DIM : (h + 1) * HEAD_DIM] for h in range(first, first + per_group)], axis=0
            )
            scores = lax.dot_general(q, k, (((1,), (1,)), ((), ())), preferred_element_type=F32) + near_bias
            sink = jnp.zeros((per_group * WINDOW, 1), F32)
            for e in range(per_group):
                sink = jnp.where(row_head == e, sink_row[:, first + e : first + e + 1], sink)
            largest = jnp.maximum(jnp.max(scores, axis=-1, keepdims=True), sink)
            powers = jnp.exp(scores - largest)
            total = jnp.sum(powers, axis=-1, keepdims=True) + jnp.exp(sink - largest)
            mixed = jnp.dot(powers.astype(BF16), v, preferred_element_type=F32) * (1.0 / total)
            mixed = mixed.astype(BF16)
            out[here, first * HEAD_DIM : (first + per_group) * HEAD_DIM] = jnp.concatenate(
                [mixed[e * WINDOW : (e + 1) * WINDOW] for e in range(per_group)], axis=1
            )

    def attend0(i):
        if i == 0:
            pl.when(span_low)(lambda: halo(0, 0, True).wait_recv())
        if i == n_tp - 1:
            pl.when(span_high)(lambda: halo(0, 0, False).wait_recv())

        def one(b, carry):
            here = pl.ds(pl.multiple_of(b * WINDOW, WINDOW), WINDOW)
            near = pl.ds(pl.multiple_of(i * tokens + b * WINDOW, WINDOW), reach_of)
            attend_block(0, queries.at[i], kv0, here, near, bias[i * blocks + b], sink_ref[0:1], mine.at[i])
            return carry

        lax.fori_loop(0, blocks, one, 0)

    def slice_copy(i, source):
        to = {"sp": sp, "tp": i}
        return send(mine.at[i], attended.at[source], slice_send.at[i], slice_recv.at[source], to)

    def send_slice(i):
        pl.when(tp != i)(lambda: slice_copy(i, tp).start())

        @pl.when(tp == i)
        def _():
            attended[i] = mine[i]

    def wait_slices():
        for t in range(n_tp):
            pl.when(tp != t)(lambda: slice_copy(t, t).wait_recv())

    def attend(layer, t):
        wait_halo(layer, t)

        def one(b, carry):
            here = pl.ds(pl.multiple_of(b * WINDOW, WINDOW), WINDOW)
            near = pl.ds(pl.multiple_of(b * WINDOW, WINDOW), reach_of)
            attend_block(
                layer, queries.at[t], kv.at[layer - 1, t], here, near, bias[tp * blocks + b],
                sinks[t, layer : layer + 1], attended.at[t],
            )
            return carry

        lax.fori_loop(0, blocks, one, 0)

    def make_state(layer, s):
        piece = jnp.zeros((tokens, rows), F32)
        for t in range(n_tp):
            piece += lax.dot_general(
                attended[t], w[2, layer, t // n_c, t % n_c, s // n_y, s % n_y],
                (((1,), (1,)), ((), ())), preferred_element_type=F32,
            )
        target = out_ref if layer == layers - 1 else state
        target[:, s * rows : (s + 1) * rows] = piece.astype(BF16)

    def sinks_here():
        for k in range(1, n_tp):
            sink_copy(k, True).wait_recv()

    work, costs = [], []

    def add(layer, kind, cost, piece, *where, after=None):
        work.append(functools.partial(piece, *where))
        costs.append((layer, kind, cost, after))
        return len(work) - 1

    for i in range(n_tp):
        add(0, None, 1.1, norm0, i)
    ends_first = [0, n_tp - 1] + list(range(1, n_tp - 1))
    for i in ends_first:
        add(0, 0, 0.85, make_kv0, i)
    sent = add(0, 0, 0.05, send_halo, 0, 0)
    for i in range(n_tp):
        add(0, 1, 0.85, make_q0, i)
    middle_first = list(range(1, n_tp)) + [0]
    for j, i in enumerate(middle_first):
        edge = i in (0, n_tp - 1)
        add(0, 1, 1.3, attend0, i, after=(sent, 5.0) if edge else None)
        if j:
            add(0, 1, 0.05, send_slice, middle_first[j - 1])
    add(0, 1, 0.05, sinks_here)
    sent = add(0, 1, 0.05, send_slice, middle_first[-1])
    add(0, 2, 0.05, wait_slices, after=(sent, 4.0))
    for layer in range(layers):
        if layer:
            add(layer, None, 1.0, norm, layer)
            sent = []
            for t in range(n_tp):
                add(layer, 0, 0.75, make_kv, layer, t)
                if t:
                    sent.append(add(layer, 0, 0.05, send_halo, layer, t - 1))
            for t in range(n_tp):
                add(layer, 1, 0.75, make_q, layer, t)
                if t == 0:
                    sent.append(add(layer, 1, 0.05, send_halo, layer, n_tp - 1))
            for t in range(n_tp):
                add(layer, 1, 1.3, attend, layer, t, after=(sent[t], 5.0))
        for s in range(n_sp):
            add(layer, 2, 0.4, make_state, layer, s)

    missing = {(layer, kind): 0 for layer in range(layers) for kind in (None, 0, 1, 2)}
    for unit in units:
        missing[unit[:2]] += 1

    def compute(budget):
        while work and missing[costs[0][:2]] == 0 and budget > 0:
            work.pop(0)()
            budget -= min(1.0, 2.0 * costs.pop(0)[2])

    def landed(u):
        missing[units[u][:2]] -= 1

    compute(n_tp)
    for s in range(count + LAGS[5] + 1):
        slots = SLOTS if s < LATE_FROM * count else LATE
        if AHEAD <= s + AHEAD < count:
            depart(s + AHEAD)
        for stage in range(3):
            u, v = s - LAGS[2 * stage], s - LAGS[2 * stage + 1]
            if 0 <= u < count:
                pass_on(u, stage)
            if 0 <= v < count:
                advance(v, stage)
                if stage == 1 and len(units[v][4][0]) == 2:
                    landed(v)
            compute(slots[stage])
        u = s - LAGS[5] - 1
        if 0 <= u < count and len(units[u][4][0]) == 3:
            wait_shared(u)
            landed(u)
        compute(slots[3])
        u = s - LAGS[5] - 1 - SETTLE
        if 0 <= u < count:
            drain(u)
    compute(math.inf)

    for u in range(count - SETTLE, count):
        drain(u)
    for k in range(1, n_tp):
        sink_copy(k, False).wait_send()
    for i in range(n_tp):
        pl.when(tp != i)(lambda: slice_copy(i, tp).wait_send())
    for layer in range(layers):
        low, high = low_high(layer)
        for t in range(n_tp if layer else 1):
            pl.when(low)(lambda: halo(layer, t, False).wait_send())
            pl.when(high)(lambda: halo(layer, t, True).wait_send())


def shards(
    grid, inputs, norm_gain, query_weight, key_weight, value_weight, output_weight, sink_logit, final_gain
):
    n_z, n_y, n_x, n_c = grid
    n_sp, n_tp = n_z * n_y, n_x * n_c
    layers, rows, cols = query_weight.shape
    kv_cols = key_weight.shape[2]
    features = inputs.shape[1]
    span = inputs.shape[0]
    tokens = span // n_tp
    units = unit_list(layers, rows)

    half = HEAD_DIM // 2
    inverse = 10000.0 ** (-jnp.arange(half).astype(F32) / half)
    inverse = jnp.tile(inverse, 4)[None]

    if kv_cols % LANES:
        weights = [jnp.concatenate([key_weight, value_weight], axis=2), query_weight, output_weight]
        sources = [(0, 0, cols), (1, 0, cols), (2, 0, cols)]
    else:
        weights = [key_weight, value_weight, query_weight, output_weight]
        sources = [(0, 0, kv_cols), (0, kv_cols, kv_cols), (1, 0, cols), (2, 0, cols)]

    copies = len(units) * (n_z + n_y + n_x - 2 + max(n_z, n_y, n_x))
    vmem = pl.BlockSpec(memory_space=pltpu.VMEM)
    hbm = pl.BlockSpec(memory_space=pl.ANY)
    state = pl.pallas_call(
        functools.partial(stack_kernel, grid, sources, units),
        name="stack",
        out_shape=jax.ShapeDtypeStruct((tokens, features), BF16),
        in_specs=[hbm, vmem, vmem, vmem] + [hbm] * len(weights),
        out_specs=vmem,
        scratch_shapes=[
            pltpu.VMEM((KINDS, layers, n_x, n_c, n_z, n_y, rows, cols), BF16),
            pltpu.VMEM((2, tokens, features), BF16),
            pltpu.VMEM((tokens, features), BF16),
            pltpu.VMEM((n_tp, tokens, features), BF16),
            pltpu.VMEM((n_tp, tokens, cols), BF16),
            pltpu.VMEM((span + 2 * WINDOW, cols), BF16),
            pltpu.VMEM((layers - 1, n_tp, tokens + 2 * WINDOW, cols), BF16),
            pltpu.VMEM((n_tp, tokens, cols), BF16),
            pltpu.VMEM((n_tp, tokens, cols), BF16),
            pltpu.VMEM((span // WINDOW, WINDOW, 3 * WINDOW), F32),
            pltpu.VMEM((span, 2 * HEAD_DIM), F32),
            pltpu.VMEM((4, tokens, cols), F32),
            pltpu.VMEM((n_tp,) + sink_logit.shape, F32),
            pltpu.SemaphoreType.DMA((copies,)),
            pltpu.SemaphoreType.DMA((copies,)),
            pltpu.SemaphoreType.DMA((layers * n_tp * 2,)),
            pltpu.SemaphoreType.DMA((layers * n_tp * 2,)),
            pltpu.SemaphoreType.DMA((n_tp,)),
            pltpu.SemaphoreType.DMA((n_tp,)),
            pltpu.SemaphoreType.DMA((n_tp - 1,)),
            pltpu.SemaphoreType.DMA((n_tp - 1,)),
            pltpu.SemaphoreType.DMA((len(weights) + n_tp,)),
        ],
        compiler_params=pltpu.CompilerParams(
            vmem_limit_bytes=VMEM_LIMIT, collective_id=0, has_side_effects=True
        ),
    )(inputs, norm_gain, sink_logit, inverse, *weights)
    step = min(64, tokens)
    return pl.pallas_call(
        finish_kernel,
        name="finish",
        grid=(tokens // step,),
        out_shape=jax.ShapeDtypeStruct((tokens, features), F32),
        in_specs=[pl.BlockSpec((step, features), lambda i: (i, 0)), pl.BlockSpec((1, features), lambda i: (0, 0))],
        out_specs=pl.BlockSpec((step, features), lambda i: (i, 0)),
    )(state, final_gain[None])


def solution(mesh):
    in_specs = (
        P("sp", None),
        P(),
        P(None, "sp", "tp"),
        P(None, "sp", "tp"),
        P(None, "sp", "tp"),
        P(None, "sp", "tp"),
        P(None, "tp"),
        P(),
    )
    out_specs = P(("sp", "tp"), None)
    return jax.shard_map(
        functools.partial(shards, grid_of(mesh)), mesh=mesh, in_specs=in_specs, out_specs=out_specs, check_vma=False
    )
```

profile of v0, /device:TPU:1, one launch (start us, length us, event | category | flops | bytes accessed | tf_op | source)
XLA Modules:
  0.0 185.9 jit_solution(3012839619339883260)
XLA Ops:
  0.0 0.6 broadcast_in_dim_tile.3.refs_3_
  0.6 181.4 %stack.1.state_ref = bf16[256,2048]{1,0:T(8,128)(2,1)} custom-call(bf16[1024,2048]{1,0:T(8,128)(2,1)} %refs_0_.1, f32[3,2048]{1,0:T(4,128)} %refs_1_.1, f32[3,4]{1,0:T(4,128)} %refs_2_.1, f32[1,128]{1,0:T(1,128)} %broadcast_in_dim_tile.3.refs_3_, bf16[3,256,128]{2,1,0:T(8,128)(2,1)} %refs_4_.1, bf16[3,256,128]{2,1,0:T(8,128)(2,1)} %refs_5_.1, ...), custom_call_target="tpu_custom_call" | custom-call | tf_op jit(solution)/shard_map/stack/pallas_call | solution.py:567
  182.0 3.8 %finish.1 = f32[256,2048]{1,0:T(8,128)} custom-call(bf16[256,2048]{1,0:T(8,128)(2,1)} %stack.1.state_ref, f32[1,2048]{1,0:T(1,128)} %bitcast.1), custom_call_target="tpu_custom_call" | custom-call | tf_op jit(solution)/shard_map/finish/pallas_call | solution.py:602
  (2 shorter events, 0.0 us)
where the time goes:
time: 186 us
  Pallas kernels  185 us (99%)
    pallas_call x1, Pallas kernels, shards(): pl.pallas_call(functools.partial(stack_kernel, grid, sources, units), nam...  181 us
    pallas_call x1, Pallas kernels, shards(): pl.pallas_call(finish_kernel, name='finish', grid=(tokens // step,), out_...  3.83 us

commit v1 on v0

--- a/solution.py
+++ b/solution.py
@@ -16,13 +16,13 @@
 BF16 = jnp.bfloat16
 VMEM_LIMIT = 60 * 1024 * 1024
 KINDS = 3
-SPLIT = 4
+SPLIT = 2
 AHEAD = 2
 LAGS = (0, 1, 2, 3, 4, 5)
-SLOTS = (0, 1, 0, 1)
-LATE = (1, 1, 1, 1)
+SLOTS = (1, 1, 0, 1)
+LATE = (2, 2, 2, 2)
 LATE_FROM = 0.75
-SETTLE = 4
+SETTLE = 2
 WHOLE = slice(None)
 LINE = 4
 
@@ -40,8 +40,9 @@
     n = 0
     for layer in range(layers):
         for kind in range(KINDS):
-            for piece in range(SPLIT):
-                size = rows // SPLIT
+            pieces = SPLIT * 2 if (layer, kind) == (layers - 1, KINDS - 1) else SPLIT
+            size = rows // pieces
+            for piece in range(pieces):
                 if layer == 0 and kind < 2:
                     orders = (("z", "y"), ("z", "y"))
                 else:

time: 186 us -> 177 us (0.952)
  Pallas kernels: 185 us -> 176 us
    pallas_call x1, Pallas kernels: 181 us -> 172 us  [shards(): pl.pallas_call(functools.partial(stack_kernel, grid, sources, units), nam...]
where the time goes in v1:
time: 177 us
  Pallas kernels  176 us (99%)
    pallas_call x1, Pallas kernels, shards(): pl.pallas_call(functools.partial(stack_kernel, grid, sources, units), nam...  172 us
    pallas_call x1, Pallas kernels, shards(): pl.pallas_call(finish_kernel, name='finish', grid=(tokens // step,), out_...  3.83 us

profile of v1, /device:TPU:1, one launch (start us, length us, event | category | flops | bytes accessed | tf_op | source)
XLA Modules:
  0.0 176.7 jit_solution(7095735588633484383)
XLA Ops:
  0.0 0.6 broadcast_in_dim_tile.3.refs_3_
  0.6 172.2 %stack.1.state_ref = bf16[256,2048]{1,0:T(8,128)(2,1)} custom-call(bf16[1024,2048]{1,0:T(8,128)(2,1)} %refs_0_.1, f32[3,2048]{1,0:T(4,128)} %refs_1_.1, f32[3,4]{1,0:T(4,128)} %refs_2_.1, f32[1,128]{1,0:T(1,128)} %broadcast_in_dim_tile.3.refs_3_, bf16[3,256,128]{2,1,0:T(8,128)(2,1)} %refs_4_.1, bf16[3,256,128]{2,1,0:T(8,128)(2,1)} %refs_5_.1, ...), custom_call_target="tpu_custom_call" | custom-call | tf_op jit(solution)/shard_map/stack/pallas_call | solution.py:568
  172.8 3.8 %finish.1 = f32[256,2048]{1,0:T(8,128)} custom-call(bf16[256,2048]{1,0:T(8,128)(2,1)} %stack.1.state_ref, f32[1,2048]{1,0:T(1,128)} %bitcast.1), custom_call_target="tpu_custom_call" | custom-call | tf_op jit(solution)/shard_map/finish/pallas_call | solution.py:603
  (2 shorter events, 0.0 us)
